TPU v7x, 256 devices: a whole 4x4x8 slice. The times are simulated.
256 devices in a mesh: sp: 32 (over z, x), dp: 8 (over y, core).
Axes of the slice: x: 4, y: 4, z: 8, core: 2. Of those that a mesh axis runs over, the one named last changes fastest.
Arguments:
- gate_in: bfloat16 [8, 16384, 4096], P('dp', 'sp'), may hold values from -6 to 6
- value_in: bfloat16 [8, 16384, 4096], P('dp', 'sp'), may hold values from -6 to 6
- segments: int32 [8, 16384], P('dp', 'sp'), may hold values from 0 to 7, never falling along the last dimension, each value on 1 to 3072 neighbouring positions
- value_gain: bfloat16 [4096], P('sp'), may hold values from 0.099609375 to 1.8984375
- mixing: bfloat16 [32, 1024, 1024], P('sp', 'dp'), may hold values from -0.1875 to 0.1875
- mixing_bias: bfloat16 [32, 1024], P('sp'), may hold values from 0.099609375 to 1.8984375
Outputs:
- gated: bfloat16 [8, 16384, 4096], P('dp', 'sp')
Inputs may be any that keep to these rules, and one draw needn't show every extreme that they name: `segments`: within each sequence the numbers never fall, every number 0 to 7 occurs, a document spans at most 3072 positions and some document spans exactly that.
All inputs are finite; a program needn't handle non-finite values.
Results may differ from a plain program's by a relative error of at most 0.0054.
Values may be sent and summed in bfloat16 or wider, within the bound.
A program may use at most 128 MiB of HBM per device.

v0:
```python
import jax
import jax.numpy as jnp
from jax import lax
from jax.sharding import PartitionSpec as P

HEAD_DIM = 128


epsilon = 1e-06


def cut_along(shard, dim, count):
    lengths = shard.shape
    parts = shard.reshape(*lengths[:dim], count, lengths[dim] // count, *lengths[dim + 1 :])
    return jnp.moveaxis(parts, dim, 0)


def cut_rows(length, count):
    unit = 8 if length >= 8 * count else 1
    return [length // unit * k // count * unit for k in range(1, count)]


def laid_out(parts, dim):
    lengths = list(parts.shape[1:])
    lengths[dim] *= parts.shape[0]
    return jnp.moveaxis(parts, 0, dim).reshape(lengths)


def exchange_in_pieces(shard, axis, pieces, split_dim, concat_dim):
    parts = cut_along(shard, split_dim, lax.axis_size(axis))
    split_at = max(range(1, max(2, parts.ndim - 1)), key=lambda d: parts.shape[d])
    gathered = []
    for piece in jnp.split(parts, cut_rows(parts.shape[split_at], pieces), axis=split_at):
        if piece.size:
            gathered.append(lax.all_to_all(piece, axis, split_axis=0, concat_axis=0, tiled=True))
    return laid_out(jnp.concatenate(gathered, axis=split_at), concat_dim)


def copy_for_each(shard, axis):
    copies = jnp.broadcast_to(shard, (lax.axis_size(axis), *shard.shape))
    return lax.all_to_all(copies, axis, split_axis=0, concat_axis=0, tiled=True)


def gathered_copies(shard, axis, dim):
    parts = copy_for_each(shard, axis)
    return laid_out(parts, dim)


def head_norm(values, gain_f, head_dim):
    shaped = values.reshape(values.shape[:-1] + (values.shape[-1] // head_dim, head_dim))
    scaled = shaped * lax.rsqrt(jnp.mean(shaped * shaped, axis=-1, keepdims=True) + epsilon)
    return (scaled.reshape(values.shape) * gain_f).astype(jnp.bfloat16)


def per_device(gate_in, value_in, segments, value_gain, mixing, mixing_bias):
    sp_count = lax.axis_size("sp")
    sequences = value_in.shape[0]
    tokens = value_in.shape[1]
    length = tokens * sp_count
    block_len = mixing.shape[2]
    heads_here = mixing.shape[0]
    head_dim = HEAD_DIM
    id_tile = jnp.broadcast_to(
        segments.astype(jnp.bfloat16)[:, :, None], (sequences, tokens, sp_count)
    )
    value_heads, id_heads = (
        exchange_in_pieces(value_in, "sp", 2, 2, 1),
        exchange_in_pieces(id_tile, "sp", 2, 2, 1),
    )
    gain_f = value_gain.astype(jnp.float32)
    normed = head_norm(jax.nn.gelu(value_heads.astype(jnp.float32)), gain_f, head_dim)
    blocks = sequences * length // block_len
    value_blocks = normed.reshape(blocks, block_len, heads_here, head_dim)
    id_blocks = id_heads.reshape(blocks, block_len)
    bias_f = mixing_bias.astype(jnp.float32)
    nothing = jnp.zeros((), jnp.bfloat16)
    shard_piece = gathered_copies(mixing, "dp", 1)
    bias_rows = jnp.transpose(bias_f)[:, :, None]

    def one_block(pair_item):
        block_values, block_ids = pair_item
        same_doc = block_ids[:, None] == block_ids[None, :]
        masked = jnp.where(same_doc[None, :, :], shard_piece, nothing)
        summed = jnp.einsum(
            "hts,shd->thd", masked, block_values, preferred_element_type=jnp.float32
        )
        return (summed + bias_rows).astype(jnp.bfloat16)

    mixed = lax.map(one_block, (value_blocks, id_blocks))
    mixed = mixed.reshape(sequences, length, heads_here * head_dim)
    returned = exchange_in_pieces(mixed, "sp", 2, 1, 2)
    return (jax.nn.gelu(gate_in.astype(jnp.float32)) * returned.astype(jnp.float32)).astype(
        jnp.bfloat16
    )


def solution(mesh):
    return jax.shard_map(
        per_device,
        mesh=mesh,
        in_specs=(
            P("dp", "sp", None),
            P("dp", "sp", None),
            P("dp", "sp"),
            P("sp"),
            P("sp", "dp", None),
            P("sp", None),
        ),
        out_specs=P("dp", "sp", None),
        check_vma=False,
    )
```

profile of v0, /device:TPU:6, one launch (start us, length us, event | category | flops | bytes accessed | tf_op | source)
XLA Modules:
  0.0 374.5 jit_solution(2990902182397834703)
XLA Ops:
  2.5 11.6 %all-to-all-start.3 = ((bf16[32,2,128]{2,1,0:T(2,128)(2,1)}), bf16[32,2,128]{2,1,0:T(2,128)(2,1)S(1)}, u32[]{:S(2)}, u32[]{:S(2)}) async-start(bf16[32,2,128]{2,1,0:T(2,128)(2,1)} %reshape.325), calls=%async_computation.3 | async-start | bytes 32768 | tf_op jit(solution)/shard_map/all_to_all | solution.py:35
  14.1 6.4 %copy.28 = bf16[1,512,4096]{1,2,0:T(8,128)(2,1)} copy(bf16[1,512,4096]{2,1,0:T(8,128)(2,1)} %param.9) | data formatting | bytes 8388608 | tf_op args[1]
  22.1 9.5 %all-to-all-start.2 = ((bf16[32,2,128]{2,1,0:T(2,128)(2,1)}), bf16[32,2,128]{2,1,0:T(2,128)(2,1)S(1)}, u32[]{:S(2)}, u32[]{:S(2)}) async-start(bf16[32,2,128]{2,1,0:T(2,128)(2,1)} %reshape.327), calls=%async_computation.2 | async-start | bytes 32768 | tf_op jit(solution)/shard_map/all_to_all | solution.py:35
  31.5 4.0 %fusion.48 = (bf16[32,1,256,128]{2,3,0,1:T(8,128)(2,1)S(1)}, bf16[32,1,256,128]{2,3,0,1:T(8,128)(2,1)}) fusion(bf16[32,1,512,128]{2,3,0,1:T(8,128)(2,1)} %bitcast.68), kind=kLoop, calls=%fused_computation.57 | loop fusion | bytes 8388608 | tf_op jit(solution)/shard_map/split | solution.py:33
  35.5 2.9 copy.29
  39.5 8.6 %all-to-all-start = ((bf16[32,1,256,128]{3,2,1,0:T(8,128)(2,1)}), bf16[32,1,256,128]{3,2,1,0:T(8,128)(2,1)S(1)}, u32[]{:S(2)}, u32[]{:S(2)}) async-start(bf16[32,1,256,128]{3,2,1,0:T(8,128)(2,1)} %copy.29), calls=%async_computation | async-start | bytes 4194304 | tf_op jit(solution)/shard_map/all_to_all | solution.py:35
  48.2 4.1 %copy.30 = bf16[32,1,256,128]{3,2,1,0:T(8,128)(2,1)} copy(bf16[32,1,256,128]{2,3,0,1:T(8,128)(2,1)} %get-tuple-element.55) | data formatting | bytes 4194304 | tf_op jit(solution)/shard_map/split | solution.py:33
  52.2 45.3 %all-to-all-done = bf16[32,1,256,128]{3,2,1,0:T(8,128)(2,1)S(1)} async-done(((bf16[32,1,256,128]{3,2,1,0:T(8,128)(2,1)}), bf16[32,1,256,128]{3,2,1,0:T(8,128)(2,1)S(1)}, u32[]{:S(2)}, u32[]{:S(2)}) %all-to-all-start) | async-done | bytes 2097184 | tf_op jit(solution)/shard_map/all_to_all | solution.py:35
  97.6 5.6 %all-to-all-start.1 = ((bf16[32,1,256,128]{3,2,1,0:T(8,128)(2,1)}), bf16[32,1,256,128]{3,2,1,0:T(8,128)(2,1)}, u32[]{:S(2)}, u32[]{:S(2)}) async-start(bf16[32,1,256,128]{3,2,1,0:T(8,128)(2,1)} %copy.30), calls=%async_computation.1 | async-start | bytes 4194304 | tf_op jit(solution)/shard_map/all_to_all | solution.py:35
  103.5 47.8 %all-to-all-done.1 = bf16[32,1,256,128]{3,2,1,0:T(8,128)(2,1)} async-done(((bf16[32,1,256,128]{3,2,1,0:T(8,128)(2,1)}), bf16[32,1,256,128]{3,2,1,0:T(8,128)(2,1)}, u32[]{:S(2)}, u32[]{:S(2)}) %all-to-all-start.1) | async-done | bytes 2097184 | tf_op jit(solution)/shard_map/all_to_all | solution.py:35
  153.0 4.5 %all-to-all-start.4 = ((bf16[8,1,128,1024]{3,2,1,0:T(8,128)(2,1)}), bf16[8,1,128,1024]{3,2,1,0:T(8,128)(2,1)}, u32[]{:S(2)}, u32[]{:S(2)}) async-start(bf16[8,1,128,1024]{3,2,1,0:T(8,128)(2,1)} %broadcast_in_dim.11), calls=%async_computation.4 | async-start | bytes 4194304 | tf_op jit(solution)/shard_map/all_to_all | solution.py:41
  157.4 4.7 %fusion.47 = f32[32,512]{1,0:T(8,128)S(1)} fusion(bf16[32,1,256,128]{3,2,1,0:T(8,128)(2,1)} %all-to-all-done.1, bf16[32,1,256,128]{3,2,1,0:T(8,128)(2,1)S(1)} %all-to-all-done), kind=kLoop, calls=%fused_computation.47 | loop fusion | flops 29343744 | bytes 4259840 | tf_op jit(solution)/shard_map/reduce_sum | solution.py:51
  164.8 5.4 %fusion.31 = bf16[16,1024,1,128]{3,1,2,0:T(8,128)(2,1)} fusion(f32[16,1024,1,128]{3,1,2,0:T(8,128)S(1)} %bitcast.67, f32[128]{0:T(128)S(1)} %convert_element_type.82, f32[16,1024]{1,0:T(8,128)S(1)} %rsqrt.12), kind=kLoop, calls=%fused_computation.31 | loop fusion | flops 23068672 | bytes 12648960 | tf_op jit(solution)/shard_map/convert_element_type | solution.py:52
  170.2 14.5 %all-to-all-done.4 = bf16[8,1,128,1024]{3,2,1,0:T(8,128)(2,1)} async-done(((bf16[8,1,128,1024]{3,2,1,0:T(8,128)(2,1)}), bf16[8,1,128,1024]{3,2,1,0:T(8,128)(2,1)}, u32[]{:S(2)}, u32[]{:S(2)}) %all-to-all-start.4) | async-done | bytes 2097184 | tf_op jit(solution)/shard_map/all_to_all | solution.py:41
  184.7 56.7 %while.10 = (s32[]{:T(128)}, bf16[16,1024,1,128]{3,1,0,2:T(8,128)(2,1)}, bf16[16,1024,1,128]{3,1,2,0:T(8,128)(2,1)}, bf16[16,1024]{1,0:T(8,128)(2,1)S(1)}, bf16[...) while((s32[]{:T(128)}, bf16[16,1024,1,128]{3,1,0,2:T(8,128)(2,1)}, ...), condition=%wide.region_2.3_spmd, body=%wide.region_1.2_spmd.sunk | while | flops 270794752 | bytes 3683409 | solution.py:89
  184.7 2.6 fusion.54
  188.3 2.6 fusion.54
  198.9 2.6 fusion.54
  202.4 2.6 fusion.54
  206.0 2.6 fusion.54
  216.6 2.6 fusion.54
  230.8 2.6 fusion.54
  241.4 4.1 %slice_bitcast_fusion.1 = (bf16[32,1,256,128]{3,2,1,0:T(8,128)(2,1)S(1)}, bf16[32,1,256,128]{3,2,1,0:T(8,128)(2,1)}) fusion(bf16[32,1,512,128]{3,2,0,1:T(8,128)(2,1)} %bitcast.69), kind=kLoop, calls=%fused_computation.51 | loop fusion | bytes 8388608 | tf_op jit(solution)/shard_map/split | solution.py:33
  245.5 56.4 %all_to_all.35 = bf16[32,1,256,128]{3,2,1,0:T(8,128)(2,1)} all-to-all(bf16[32,1,256,128]{3,2,1,0:T(8,128)(2,1)S(1)} %get-tuple-element.52), channel_id=1, replica_groups=mesh['sp'=32,'dp'=8] {'sp'}, dimensions={0} | all-to-all | bytes 4194304 | tf_op jit(solution)/shard_map/all_to_all | solution.py:35
  301.9 5.6 %all-to-all-start.6 = ((bf16[32,1,256,128]{3,2,1,0:T(8,128)(2,1)}), bf16[32,1,256,128]{3,2,1,0:T(8,128)(2,1)S(1)}, u32[]{:S(2)}, u32[]{:S(2)}) async-start(bf16[32,1,256,128]{3,2,1,0:T(8,128)(2,1)} %get-tuple-element.53), calls=%async_computation.6 | async-start | bytes 4194304 | tf_op jit(solution)/shard_map/all_to_all | solution.py:35
  307.4 6.4 %copy.27 = bf16[1,512,4096]{1,2,0:T(8,128)(2,1)} copy(bf16[1,512,4096]{2,1,0:T(8,128)(2,1)} %param.8) | data formatting | bytes 8388608 | tf_op args[0]
  313.8 4.1 %copy.39 = bf16[32,1,256,128]{2,3,0,1:T(8,128)(2,1)} copy(bf16[32,1,256,128]{3,2,1,0:T(8,128)(2,1)} %all_to_all.35) | data formatting | bytes 4194304 | tf_op jit(solution)/shard_map/all_to_all | solution.py:35
  317.9 38.8 %all-to-all-done.6 = bf16[32,1,256,128]{3,2,1,0:T(8,128)(2,1)S(1)} async-done(((bf16[32,1,256,128]{3,2,1,0:T(8,128)(2,1)}), bf16[32,1,256,128]{3,2,1,0:T(8,128)(2,1)S(1)}, u32[]{:S(2)}, u32[]{:S(2)}) %all-to-all-start.6) | async-done | bytes 2097184 | tf_op jit(solution)/shard_map/all_to_all | solution.py:35
  356.7 2.9 copy.40
  359.6 3.6 maximum_convert_fusion.1
  363.2 5.0 %fusion.46 = bf16[1,512,4096]{1,2,0:T(8,128)(2,1)} fusion(bf16[1,512,4096]{1,2,0:T(8,128)(2,1)S(1)} %copy-done, f32[32,1,512,128]{2,3,0,1:T(8,128)S(1)} %maximum_convert_fusion.1), kind=kLoop, calls=%fused_computation.46 | loop fusion | flops 23068672 | bytes 16777216 | tf_op jit(solution)/shard_map/convert_element_type | solution.py:92
  368.2 6.3 %copy.41 = bf16[1,512,4096]{2,1,0:T(8,128)(2,1)} copy(bf16[1,512,4096]{1,2,0:T(8,128)(2,1)} %fusion.46) | data formatting | bytes 8388608 | tf_op jit(solution)/shard_map/convert_element_type | solution.py:92
  (87 shorter events, 47.9 us)
Async XLA Ops:
  2.5 19.6 %all-to-all-start.3 = ((bf16[32,2,128]{2,1,0:T(2,128)(2,1)}), bf16[32,2,128]{2,1,0:T(2,128)(2,1)S(1)}, u32[]{:S(2)}, u32[]{:S(2)}) async-start(bf16[32,2,128]{2,1,0:T(2,128)(2,1)} %reshape.325), calls=%async_computation.3 | async-start | bytes 32768 | tf_op jit(solution)/shard_map/all_to_all | solution.py:35
  22.1 17.5 %all-to-all-start.2 = ((bf16[32,2,128]{2,1,0:T(2,128)(2,1)}), bf16[32,2,128]{2,1,0:T(2,128)(2,1)S(1)}, u32[]{:S(2)}, u32[]{:S(2)}) async-start(bf16[32,2,128]{2,1,0:T(2,128)(2,1)} %reshape.327), calls=%async_computation.2 | async-start | bytes 32768 | tf_op jit(solution)/shard_map/all_to_all | solution.py:35
  35.5 67.7 %copy-start.3 = (bf16[128]{0:T(256)(128)(2,1)S(1)}, bf16[128]{0:T(256)(128)(2,1)}, u32[]{:S(2)}) copy-start(bf16[128]{0:T(256)(128)(2,1)} %param.11) | copy-start | bytes 772
  35.5 67.7 %copy-start.2 = (bf16[1,1024]{1,0:T(2,128)(2,1)S(1)}, bf16[1,1024]{1,0:T(2,128)(2,1)}, u32[]{:S(2)}) copy-start(bf16[1,1024]{1,0:T(2,128)(2,1)} %param.13) | copy-start | bytes 6148
  35.5 115.8 %copy-start.1 = (bf16[1,128,1024]{2,1,0:T(8,128)(2,1)S(1)}, bf16[1,128,1024]{2,1,0:T(8,128)(2,1)}, u32[]{:S(2)}) copy-start(bf16[1,128,1024]{2,1,0:T(8,128)(2,1)} %param.12) | copy-start | bytes 786436
  39.5 58.0 %all-to-all-start = ((bf16[32,1,256,128]{3,2,1,0:T(8,128)(2,1)}), bf16[32,1,256,128]{3,2,1,0:T(8,128)(2,1)S(1)}, u32[]{:S(2)}, u32[]{:S(2)}) async-start(bf16[32,1,256,128]{3,2,1,0:T(8,128)(2,1)} %copy.29), calls=%async_computation | async-start | bytes 4194304 | tf_op jit(solution)/shard_map/all_to_all | solution.py:35
  97.6 53.8 %all-to-all-start.1 = ((bf16[32,1,256,128]{3,2,1,0:T(8,128)(2,1)}), bf16[32,1,256,128]{3,2,1,0:T(8,128)(2,1)}, u32[]{:S(2)}, u32[]{:S(2)}) async-start(bf16[32,1,256,128]{3,2,1,0:T(8,128)(2,1)} %copy.30), calls=%async_computation.1 | async-start | bytes 4194304 | tf_op jit(solution)/shard_map/all_to_all | solution.py:35
  153.0 31.7 %all-to-all-start.4 = ((bf16[8,1,128,1024]{3,2,1,0:T(8,128)(2,1)}), bf16[8,1,128,1024]{3,2,1,0:T(8,128)(2,1)}, u32[]{:S(2)}, u32[]{:S(2)}) async-start(bf16[8,1,128,1024]{3,2,1,0:T(8,128)(2,1)} %broadcast_in_dim.11), calls=%async_computation.4 | async-start | bytes 4194304 | tf_op jit(solution)/shard_map/all_to_all | solution.py:41
  301.9 54.8 %all-to-all-start.6 = ((bf16[32,1,256,128]{3,2,1,0:T(8,128)(2,1)}), bf16[32,1,256,128]{3,2,1,0:T(8,128)(2,1)S(1)}, u32[]{:S(2)}, u32[]{:S(2)}) async-start(bf16[32,1,256,128]{3,2,1,0:T(8,128)(2,1)} %get-tuple-element.53), calls=%async_computation.6 | async-start | bytes 4194304 | tf_op jit(solution)/shard_map/all_to_all | solution.py:35
  359.6 3.6 copy-start
where the time goes:
time: 376 us; the launch traced here: 374 us
  waiting for transfers between devices  148 us (39%)
  local copies, waits for them, and re-layouts  59.3 us (16%)
  blocking collectives  56.4 us (15%)
  starting transfers between devices  45.3 us (12%)
  matrix products  41.7 us (11%)
  other arithmetic  23.4 us (6%)
    all_to_all x5, waiting for transfers between devices, exchange_in_pieces(): lax.all_to_all(piece, axis, split_axis=0, concat_axis=0, tiled=True)  133 us
    all_to_all x1, blocking collectives, exchange_in_pieces(): lax.all_to_all(piece, axis, split_axis=0, concat_axis=0, tiled=True)  56.4 us
    dot_general x16, matrix products, one_block(): jnp.einsum('hts,shd->thd', masked, block_values, preferred_element_type=j...  41.7 us
    all_to_all x5, starting transfers between devices, exchange_in_pieces(): lax.all_to_all(piece, axis, split_axis=0, concat_axis=0, tiled=True)  40.9 us
    split x5, local copies, waits for them, and re-layouts, exchange_in_pieces(): jnp.split(parts, cut_rows(parts.shape[split_at], pieces), axis=split_at)  15 us
    unnamed x17, local copies, waits for them, and re-layouts  14.6 us
    all_to_all x1, waiting for transfers between devices, copy_for_each(): return lax.all_to_all(copies, axis, split_axis=0, concat_axis=0, tiled=True)  14.5 us
    dynamic_update_slice x32, local copies, waits for them, and re-layouts, per_device(): mixed = lax.map(one_block, (value_blocks, id_blocks))  14.3 us
  transfers between devices with their start and end apart: 6, of which 6 were waited for; matrix products, arithmetic and copies ran while one was open for 11% of the time, Pallas kernels for 0%

commit v1 on v0

v1 whole, which is shorter than its diff:
```python
import jax
import jax.numpy as jnp
from jax import lax
from jax.experimental import pallas as pl
from jax.experimental.pallas import tpu as pltpu
from jax.sharding import PartitionSpec as P

MESH = pl.DeviceIdType.MESH
EPSILON = 1e-06
BF16, F32 = jnp.bfloat16, jnp.float32
NX, NY, NZ, NC = 4, 4, 8, 2
HD = 128
TOK = 512
BLK = 1024
HALF = 64
STEPS = 8


def gelu(x):
    inner = 0.7978845608028654 * (x + 0.044715 * (x * x * x))
    return x * (0.5 * (1.0 + jnp.tanh(inner)))


def kernel(
    gate_hbm,
    value_hbm,
    seg_hbm,
    aux_hbm,
    mix_hbm,
    out_ref,
    m_buf,
    v_buf,
    r_buf,
    o_buf,
    g_buf,
    mask_buf,
    vn_buf,
    col_buf,
    seg_buf,
    aux_buf,
    loc_sem,
    own_v_sem,
    seg_s,
    seg_r,
    v_s,
    v_r,
    r_s,
    r_r,
    a1_s,
    a1_r,
    a_s,
    a_r,
    b_s,
    b_r,
    x_s,
    x_r,
    b2_s,
    b2_r,
    c_s,
    c_r,
):
    sp, dp = lax.axis_index("sp"), lax.axis_index("dp")
    z, x = sp // NX, lax.rem(sp, NX)
    y, c = dp // NC, lax.rem(dp, NC)

    def x_peer(j):
        return {"sp": z * NX + lax.rem(x + j, NX), "dp": dp}

    def y_peer(j):
        return {"sp": sp, "dp": lax.rem(y + j, NY) * NC + c}

    def z_peer(j):
        return {"sp": lax.rem(z + j, NZ) * NX + x, "dp": dp}

    sibling = {"sp": sp, "dp": y * NC + (1 - c)}

    def remote(src, dst, ss, rs, dev):
        return pltpu.make_async_remote_copy(
            src_ref=src, dst_ref=dst, send_sem=ss, recv_sem=rs, device_id=dev, device_id_type=MESH
        )

    def head_z(k):
        far = (k + 1) // 2
        return lax.rem(z + jnp.where(lax.rem(k, 2) == 1, far, NZ - far), NZ)

    def head_cols(k, xs):
        return pl.ds(pl.multiple_of((head_z(k) * NX + xs) * HD, HD), HD)

    def x_rows(xs):
        return pl.ds(pl.multiple_of(xs * TOK, TOK), TOK)

    def v_send(k, j):
        xs = lax.rem(x + j, NX)
        return remote(
            value_hbm.at[0, :, head_cols(k, xs)],
            v_buf.at[k, x_rows(x)],
            v_s.at[k, j - 1],
            v_r.at[k, j - 1],
            x_peer(j),
        )

    def v_recv(k, j):
        xs = lax.rem(x + NX - j, NX)
        return remote(
            v_buf.at[k, x_rows(xs)], v_buf.at[k, x_rows(xs)], v_s.at[k, j - 1], v_r.at[k, j - 1], x_peer(j)
        )

    def r_send(k, j):
        xs = lax.rem(x + j, NX)
        return remote(
            r_buf.at[k, x_rows(xs)], o_buf.at[x, k], r_s.at[k, j - 1], r_r.at[k, j - 1], x_peer(j)
        )

    def r_recv(k, j):
        xs = lax.rem(x + NX - j, NX)
        return remote(o_buf.at[xs, k], o_buf.at[xs, k], r_s.at[k, j - 1], r_r.at[k, j - 1], x_peer(j))

    def seg_send(j):
        return remote(seg_hbm, seg_buf.at[x], seg_s.at[j - 1], seg_r.at[j - 1], x_peer(j))

    def seg_recv(j):
        xs = lax.rem(x + NX - j, NX)
        return remote(seg_buf.at[xs], seg_buf.at[xs], seg_s.at[j - 1], seg_r.at[j - 1], x_peer(j))

    def a1_send(j):
        return remote(
            mix_hbm.at[0, pl.ds(0, HALF)], m_buf.at[z, y, c, 0], a1_s.at[j - 1], a1_r.at[j - 1], y_peer(j)
        )

    def a1_recv(j):
        ref = m_buf.at[z, lax.rem(y + NY - j, NY), c, 0]
        return remote(ref, ref, a1_s.at[j - 1], a1_r.at[j - 1], y_peer(j))

    def a_msg(zh, ss, rs, dz):
        ref = m_buf.at[zh, :, c, 0]
        return remote(ref, ref, a_s.at[ss], a_r.at[rs], z_peer(dz))

    def a_half(zh, lo, ss, rs, dz):
        ref = m_buf.at[zh, pl.ds(lo, 2), c, 0]
        return remote(ref, ref, a_s.at[ss], a_r.at[rs], z_peer(dz))

    def b_msg(zh, ss, rs, dz):
        ref = m_buf.at[zh, y, c, 1]
        return remote(ref, ref, b_s.at[ss], b_r.at[rs], z_peer(dz))

    def b_half(zh, lo, ss, rs, dz):
        ref = m_buf.at[zh, y, c, 1, pl.ds(lo, HALF // 2)]
        return remote(ref, ref, b_s.at[ss], b_r.at[rs], z_peer(dz))

    def x_msg(zh, ss, rs, dz):
        ref = aux_buf.at[zh]
        return remote(ref, ref, x_s.at[ss], x_r.at[rs], z_peer(dz))

    def b2_send(k, j):
        ref = m_buf.at[head_z(k), y, c, 1]
        return remote(ref, ref, b2_s.at[k, j - 1], b2_r.at[k, j - 1], y_peer(j))

    def b2_recv(k, j):
        ref = m_buf.at[head_z(k), lax.rem(y + NY - j, NY), c, 1]
        return remote(ref, ref, b2_s.at[k, j - 1], b2_r.at[k, j - 1], y_peer(j))

    def c_send(k):
        ref = m_buf.at[head_z(k), :, c]
        return remote(ref, ref, c_s.at[k], c_r.at[k], sibling)

    def c_recv(k):
        ref = m_buf.at[head_z(k), :, 1 - c]
        return remote(ref, ref, c_s.at[k], c_r.at[k], sibling)

    barrier = pltpu.get_barrier_semaphore()
    peers = [x_peer(j) for j in (1, 2, 3)] + [y_peer(j) for j in (1, 2, 3)]
    peers += [z_peer(1), z_peer(NZ - 1), sibling]
    for peer in peers:
        pl.semaphore_signal(barrier, inc=1, device_id=peer, device_id_type=MESH)

    own_a = pltpu.make_async_copy(mix_hbm.at[0, pl.ds(0, HALF)], m_buf.at[z, y, c, 0], loc_sem.at[0])
    own_b = pltpu.make_async_copy(mix_hbm.at[0, pl.ds(HALF, HALF)], m_buf.at[z, y, c, 1], loc_sem.at[1])
    own_x = pltpu.make_async_copy(aux_hbm, aux_buf.at[z], loc_sem.at[2])
    own_seg = pltpu.make_async_copy(seg_hbm, seg_buf.at[x], loc_sem.at[3])
    own_gate = pltpu.make_async_copy(gate_hbm.at[0], g_buf, loc_sem.at[4])

    def own_v(k):
        return pltpu.make_async_copy(
            value_hbm.at[0, :, head_cols(k, x)], v_buf.at[k, x_rows(x)], own_v_sem.at[k]
        )

    own_a.start()
    own_b.start()
    own_x.start()
    own_seg.start()
    pl.semaphore_wait(barrier, len(peers))

    for j in (1, 2, 3):
        seg_send(j).start()
    for j in (1, 2, 3):
        a1_send(j).start()

    def start_v(k, carry):
        own_v(k).start()
        for j in (1, 3, 2):
            v_send(k, j).start()
        return carry

    lax.fori_loop(0, 2, start_v, 0)
    own_b.wait()
    own_x.wait()
    b_msg(z, 0, 1, NZ - 1).start()
    b_msg(z, 8, 2, 1).start()
    x_msg(z, 0, 1, NZ - 1).start()
    x_msg(z, 7, 2, 1).start()
    for j in (1, 2, 3):
        b2_send(0, j).start()
    lax.fori_loop(2, STEPS, start_v, 0)
    own_gate.start()

    own_seg.wait()
    for j in (1, 2, 3):
        seg_recv(j).wait_recv()

    def as_column(row):
        return jnp.transpose(jnp.broadcast_to(row, (HD, row.shape[1])))

    for s in range(NX):
        col_buf[pl.ds(lax.rem(s, 2) * TOK, TOK), :] = as_column(seg_buf[s].astype(F32))
        if s % 2 == 1:
            rows_ids = [seg_buf[s - 1].astype(F32), seg_buf[s].astype(F32)]

            def mask_rows(i, carry):
                rows = pl.ds(pl.multiple_of(i * 64, 64), 64)
                ids = col_buf[rows, :]
                for half in range(2):
                    for t in range(TOK // HD):
                        there = rows_ids[half][:, t * HD : (t + 1) * HD]
                        mask_buf[s // 2, rows, half * TOK + t * HD : half * TOK + (t + 1) * HD] = jnp.where(
                            ids == there, 1.0, 0.0
                        ).astype(BF16)
                return carry

            lax.fori_loop(0, BLK // 64, mask_rows, 0)

    def serve(k):
        zh = head_z(k)
        odd = lax.rem(k, 2) == 1

        @pl.when(k == 0)
        def _():
            own_a.wait()
            for j in (1, 2, 3):
                a1_recv(j).wait_recv()
            a_msg(z, 0, 1, NZ - 1).start()
            a_msg(z, 8, 2, 1).start()

        @pl.when((k >= 1) & (k <= 6))
        def _():
            a_msg(zh, k, k, 1).wait_recv()
            x_msg(zh, k, k, 1).wait_recv()
            b_msg(zh, k, k, 1).wait_recv()

        @pl.when((k >= 1) & (k <= 4))
        def _():
            dz = jnp.where(odd, NZ - 1, 1)
            a_msg(zh, k, k + 2, dz).start()
            x_msg(zh, k, k + 2, dz).start()
            b_msg(zh, k, k + 2, dz).start()

        @pl.when(k == 5)
        def _():
            a_half(zh, 0, 5, 7, NZ - 1).start()
            b_half(zh, 0, 5, 7, NZ - 1).start()
            x_msg(zh, 5, 7, NZ - 1).start()

        @pl.when(k == 6)
        def _():
            a_half(zh, 2, 6, 8, 1).start()
            b_half(zh, HALF // 2, 6, 8, 1).start()

        @pl.when(k == 7)
        def _():
            a_half(zh, 0, 7, 7, 1).wait_recv()
            a_half(zh, 2, 7, 8, 1).wait_recv()
            x_msg(zh, 7, 7, 1).wait_recv()
            b_half(zh, 0, 7, 7, 1).wait_recv()
            b_half(zh, HALF // 2, 7, 8, 1).wait_recv()

        @pl.when(k >= 1)
        def _():
            for j in (1, 2, 3):
                b2_send(k, j).start()

    def across(k):
        for j in (1, 2, 3):
            b2_recv(k, j).wait_recv()
        c_send(k).start()

    def compute(k):
        zh = head_z(k)
        own_v(k).wait()
        for j in (1, 2, 3):
            v_recv(k, j).wait_recv()
        aux = aux_buf[zh]
        gain = aux[:, BLK:]
        for t in range(BLK // TOK):
            col_buf[pl.ds(t * TOK, TOK), :] = as_column(aux[:, t * TOK : (t + 1) * TOK])

        def norm_rows(i, carry):
            rows = pl.ds(pl.multiple_of(i * 128, 128), 128)
            act = gelu(v_buf[k, rows, :].astype(F32))
            scaled = act * lax.rsqrt(jnp.mean(act * act, axis=-1, keepdims=True) + EPSILON)
            vn_buf[rows, :] = (scaled * gain).astype(BF16)
            return carry

        lax.fori_loop(0, NX * TOK // 128, norm_rows, 0)
        c_recv(k).wait_recv()

        def mix_rows(i, carry):
            block, part = i // NY, lax.rem(i, NY)
            rows = pl.ds(pl.multiple_of(part * 256, 256), 256)
            matrix = m_buf[zh, part].reshape(256, BLK) * mask_buf[block, rows, :]
            values = vn_buf[pl.ds(pl.multiple_of(block * BLK, BLK), BLK), :]
            summed = jnp.dot(matrix, values, preferred_element_type=F32)
            r_buf[k, pl.ds(pl.multiple_of(block * BLK + part * 256, 256), 256), :] = (
                summed + col_buf[rows, :]
            ).astype(BF16)
            return carry

        lax.fori_loop(0, 2 * NY, mix_rows, 0)
        for j in (1, 3, 2):
            r_send(k, j).start()

    def step(i, carry):
        @pl.when(i < STEPS)
        def _():
            serve(i)

        @pl.when((i >= 1) & (i <= STEPS))
        def _():
            across(i - 1)

        @pl.when(i >= 2)
        def _():
            compute(i - 2)

        return carry

    lax.fori_loop(0, STEPS + 2, step, 0)

    own_gate.wait()

    def gate_rows(k, xs, source):
        cols = head_cols(k, xs)
        for i in range(TOK // 128):
            rows = pl.ds(i * 128, 128)
            gate = gelu(g_buf[rows, cols].astype(F32))
            out_ref[0, rows, cols] = (gate * source(i * 128).astype(F32)).astype(BF16)

    def own_gated(k, carry):
        gate_rows(
            k, x, lambda lo: r_buf[k, pl.ds(pl.multiple_of(x * TOK + lo, 128), 128), :]
        )
        return carry

    lax.fori_loop(0, STEPS, own_gated, 0)

    def gated(k, carry):
        for j in (1, 3, 2):
            r_recv(k, j).wait_recv()
            xs = lax.rem(x + NX - j, NX)
            gate_rows(k, xs, lambda lo: o_buf[xs, k, pl.ds(lo, 128), :])
        return carry

    lax.fori_loop(0, STEPS, gated, 0)

    def sent(k, carry):
        for j in (1, 2, 3):
            v_send(k, j).wait_send()
            r_send(k, j).wait_send()
            b2_send(k, j).wait_send()
        c_send(k).wait_send()
        return carry

    lax.fori_loop(0, STEPS, sent, 0)
    for j in (1, 2, 3):
        seg_send(j).wait_send()
        a1_send(j).wait_send()
    for k in (0, 1, 2, 3, 4, 8):
        a_msg(z, k, 0, 1).wait_send()
        b_msg(z, k, 0, 1).wait_send()
    for k in (5, 6):
        a_half(z, 0, k, 0, 1).wait_send()
        b_half(z, 0, k, 0, 1).wait_send()
    for k in (0, 1, 2, 3, 4, 5, 7):
        x_msg(z, k, 0, 1).wait_send()


def per_device(gate_in, value_in, segments, value_gain, mixing, mixing_bias):
    aux = jnp.concatenate([mixing_bias.astype(F32), value_gain.astype(F32)[None, :]], axis=1)
    any_space = pl.BlockSpec(memory_space=pl.ANY)
    dma = pltpu.SemaphoreType.DMA
    return pl.pallas_call(
        kernel,
        out_shape=jax.ShapeDtypeStruct(value_in.shape, BF16),
        in_specs=[any_space] * 5,
        out_specs=pl.BlockSpec(memory_space=pltpu.VMEM),
        scratch_shapes=[
            pltpu.VMEM((NZ, NY, NC, 2, HALF, BLK), BF16),
            pltpu.VMEM((STEPS, NX * TOK, HD), BF16),
            pltpu.VMEM((STEPS, NX * TOK, HD), BF16),
            pltpu.VMEM((NX, STEPS, TOK, HD), BF16),
            pltpu.VMEM((TOK, NX * NZ * HD), BF16),
            pltpu.VMEM((2, BLK, BLK), BF16),
            pltpu.VMEM((NX * TOK, HD), BF16),
            pltpu.VMEM((BLK, HD), F32),
            pltpu.VMEM((NX, 1, TOK), jnp.int32),
            pltpu.VMEM((NZ, 1, BLK + HD), F32),
            dma((5,)),
            dma((STEPS,)),
            dma((3,)),
            dma((3,)),
            dma((STEPS, 3)),
            dma((STEPS, 3)),
            dma((STEPS, 3)),
            dma((STEPS, 3)),
            dma((3,)),
            dma((3,)),
            dma((9,)),
            dma((9,)),
            dma((9,)),
            dma((9,)),
            dma((8,)),
            dma((8,)),
            dma((STEPS, 3)),
            dma((STEPS, 3)),
            dma((STEPS,)),
            dma((STEPS,)),
        ],
        compiler_params=pltpu.CompilerParams(
            collective_id=0, has_side_effects=True, vmem_limit_bytes=60 * 1024 * 1024
        ),
    )(gate_in, value_in, segments, aux, mixing)


def solution(mesh):
    return jax.shard_map(
        per_device,
        mesh=mesh,
        in_specs=(
            P("dp", "sp", None),
            P("dp", "sp", None),
            P("dp", "sp"),
            P("sp"),
            P("sp", "dp", None),
            P("sp", None),
        ),
        out_specs=P("dp", "sp", None),
        check_vma=False,
    )
```

time: 376 us -> 110 us (0.29)
  waiting for transfers between devices: 148 us -> 0 us
  Pallas kernels: 0 us -> 102 us
  blocking collectives: 56.4 us -> 0 us
  local copies, waits for them, and re-layouts: 59.3 us -> 4.7 us
  starting transfers between devices: 45.3 us -> 0 us
  matrix products: 41.7 us -> 0 us
  other arithmetic: 23.4 us -> 1.3 us
    all_to_all x6 -> x0, waiting for transfers between devices: 148 us -> none  [the longest x5 133 us: exchange_in_pieces(): lax.all_to_all(piece, axis, split_axis=0, concat_axis=0, tiled=True)]
    pallas_call x0 -> x1, Pallas kernels: none -> 102 us  [per_device(): pl.pallas_call(kernel, out_shape=jax.ShapeDtypeStruct(value_in.shape, BF1...]
    all_to_all x1 -> x0, blocking collectives: 56.4 us -> none  [exchange_in_pieces(): lax.all_to_all(piece, axis, split_axis=0, concat_axis=0, tiled=True)]
    all_to_all x6 -> x0, starting transfers between devices: 45.3 us -> none  [the longest x5 40.9 us: exchange_in_pieces(): lax.all_to_all(piece, axis, split_axis=0, concat_axis=0, tiled=True)]
    dot_general x16 -> x0, matrix products: 41.7 us -> none  [one_block(): jnp.einsum('hts,shd->thd', masked, block_values, preferred_element_type=j...]
    convert_element_type x6 -> x0, other arithmetic: 17.2 us -> none  [the longest x1 5.41 us: head_norm(): return (scaled.reshape(values.shape) * gain_f).astype(jnp.bfloat16)]
    split x5 -> x0, local copies, waits for them, and re-layouts: 15 us -> none  [exchange_in_pieces(): jnp.split(parts, cut_rows(parts.shape[split_at], pieces), axis=split_at)]
    dynamic_update_slice x32 -> x0, local copies, waits for them, and re-layouts: 14.3 us -> none  [per_device(): mixed = lax.map(one_block, (value_blocks, id_blocks))]
  transfers between devices with their start and end apart: 6 -> 0, of which waited for: 6 -> 0; matrix products, arithmetic and copies ran while one was open for 11% -> 0% of each run, Pallas kernels for 0% -> 0%
where the time goes in v1:
time: 110 us; the launch traced here: 108 us
  Pallas kernels  102 us (93%)
  local copies, waits for them, and re-layouts  4.7 us (4%)
  other arithmetic  1.3 us (1%)
    pallas_call x1, Pallas kernels, per_device(): pl.pallas_call(kernel, out_shape=jax.ShapeDtypeStruct(value_in.shape, BF1...  102 us
    unnamed x1, local copies, waits for them, and re-layouts  4.7 us

profile of v1, /device:TPU:6, one launch (start us, length us, event | category | flops | bytes accessed | tf_op | source)
XLA Modules:
  0.0 108.2 jit_solution(14577006458245270456)
XLA Ops:
  0.0 1.3 %maximum_convert_fusion.aux_hbm = f32[1,1152]{1,0:T(1,128)} fusion(bf16[1,128]{1,0:T(2,128)(2,1)} %bitcast.1, bf16[1,1024]{1,0:T(2,128)(2,1)} %param.11), kind=kLoop, calls=%fused_computation | loop fusion | flops 4608 | bytes 6912 | tf_op jit(solution)/shard_map/concatenate | solution.py:396
  1.3 102.2 %shard_map.64 = bf16[1,512,4096]{2,1,0:T(8,128)(2,1)} custom-call(bf16[1,512,4096]{2,1,0:T(8,128)(2,1)} %gate_hbm.1, bf16[1,512,4096]{2,1,0:T(8,128)(2,1)} %value_hbm.1, s32[1,512]{1,0:T(1,128)} %seg_hbm.1, f32[1,1152]{1,0:T(1,128)} %maximum_convert_fusion.aux_hbm, bf16[1,128,1024]{2,1,0:T(8,128)(2,1)} %mix_hbm.1), custom_call_target="tpu_custom_call" | custom-call | tf_op jit(solution)/shard_map/pallas_call | solution.py:399
  103.5 4.7 %copy.8 = bf16[1,512,4096]{2,1,0:T(8,128)(2,1)} copy(bf16[1,512,4096]{2,1,0:T(8,128)(2,1)} %shard_map.64) | data formatting | bytes 8388608

commit v2 on v1

--- a/solution.py
+++ b/solution.py
@@ -25,8 +25,9 @@
     gate_hbm,
     value_hbm,
     seg_hbm,
-    aux_hbm,
+    gain_hbm,
     mix_hbm,
+    bias_hbm,
     out_ref,
     m_buf,
     v_buf,
@@ -37,7 +38,8 @@
     vn_buf,
     col_buf,
     seg_buf,
-    aux_buf,
+    bias_buf,
+    gain_buf,
     loc_sem,
     own_v_sem,
     seg_s,
@@ -52,12 +54,16 @@
     a_r,
     b_s,
     b_r,
-    x_s,
-    x_r,
+    bias_s,
+    bias_r,
+    gain_s,
+    gain_r,
     b2_s,
     b2_r,
     c_s,
     c_r,
+    row_sem,
+    far_sem,
 ):
     sp, dp = lax.axis_index("sp"), lax.axis_index("dp")
     z, x = sp // NX, lax.rem(sp, NX)
@@ -147,9 +153,12 @@
         ref = m_buf.at[zh, y, c, 1, pl.ds(lo, HALF // 2)]
         return remote(ref, ref, b_s.at[ss], b_r.at[rs], z_peer(dz))
 
-    def x_msg(zh, ss, rs, dz):
-        ref = aux_buf.at[zh]
-        return remote(ref, ref, x_s.at[ss], x_r.at[rs], z_peer(dz))
+    def x_msgs(zh, ss, rs, dz):
+        bias, gain = bias_buf.at[zh], gain_buf.at[zh]
+        return (
+            remote(bias, bias, bias_s.at[ss], bias_r.at[rs], z_peer(dz)),
+            remote(gain, gain, gain_s.at[ss], gain_r.at[rs], z_peer(dz)),
+        )
 
     def b2_send(k, j):
         ref = m_buf.at[head_z(k), y, c, 1]
@@ -168,49 +177,79 @@
         return remote(ref, ref, c_s.at[k], c_r.at[k], sibling)
 
     barrier = pltpu.get_barrier_semaphore()
-    peers = [x_peer(j) for j in (1, 2, 3)] + [y_peer(j) for j in (1, 2, 3)]
-    peers += [z_peer(1), z_peer(NZ - 1), sibling]
-    for peer in peers:
-        pl.semaphore_signal(barrier, inc=1, device_id=peer, device_id_type=MESH)
+
+    def tell(peer, core):
+        there = {"sp": peer["sp"], "dp": peer["dp"] // NC * NC + core}
+        pl.semaphore_signal(barrier, inc=1, device_id=there, device_id_type=MESH)
+
+    @pl.when(c == 0)
+    def _():
+        pl.semaphore_signal(barrier, inc=1, device_id=sibling, device_id_type=MESH)
+
+    for j in (1, 2, 3):
+        tell(x_peer(j), 1)
+    for peer in [z_peer(1), z_peer(NZ - 1)] + [y_peer(j) for j in (1, 2, 3)]:
+        tell(peer, 0)
 
     own_a = pltpu.make_async_copy(mix_hbm.at[0, pl.ds(0, HALF)], m_buf.at[z, y, c, 0], loc_sem.at[0])
     own_b = pltpu.make_async_copy(mix_hbm.at[0, pl.ds(HALF, HALF)], m_buf.at[z, y, c, 1], loc_sem.at[1])
-    own_x = pltpu.make_async_copy(aux_hbm, aux_buf.at[z], loc_sem.at[2])
+    own_bias = pltpu.make_async_copy(bias_hbm, bias_buf.at[z], loc_sem.at[2])
     own_seg = pltpu.make_async_copy(seg_hbm, seg_buf.at[x], loc_sem.at[3])
     own_gate = pltpu.make_async_copy(gate_hbm.at[0], g_buf, loc_sem.at[4])
+    own_gain = pltpu.make_async_copy(gain_hbm, gain_buf.at[z], loc_sem.at[5])
 
     def own_v(k):
         return pltpu.make_async_copy(
             value_hbm.at[0, :, head_cols(k, x)], v_buf.at[k, x_rows(x)], own_v_sem.at[k]
         )
 
-    own_a.start()
-    own_b.start()
-    own_x.start()
-    own_seg.start()
-    pl.semaphore_wait(barrier, len(peers))
-
-    for j in (1, 2, 3):
-        seg_send(j).start()
-    for j in (1, 2, 3):
-        a1_send(j).start()
+    for own in (own_b, own_a, own_bias, own_gain, own_seg):
+        own.start()
+
+    @pl.when(c == 1)
+    def _():
+        pl.semaphore_wait(barrier, 7)
+        pl.semaphore_signal(row_sem, inc=1, device_id=sibling, device_id_type=MESH)
+
+    @pl.when(c == 0)
+    def _():
+        pl.semaphore_wait(row_sem, 1)
 
     def start_v(k, carry):
-        own_v(k).start()
         for j in (1, 3, 2):
             v_send(k, j).start()
         return carry
 
-    lax.fori_loop(0, 2, start_v, 0)
+    def start_own_v(k, carry):
+        own_v(k).start()
+        return carry
+
+    lax.fori_loop(0, 1, start_v, 0)
+    for j in (1, 2, 3):
+        seg_send(j).start()
+    lax.fori_loop(1, STEPS, start_v, 0)
+
+    @pl.when(c == 0)
+    def _():
+        pl.semaphore_wait(barrier, 10)
+        pl.semaphore_signal(far_sem, inc=1, device_id=sibling, device_id_type=MESH)
+
+    @pl.when(c == 1)
+    def _():
+        pl.semaphore_wait(far_sem, 1)
+
+    for j in (1, 2, 3):
+        a1_send(j).start()
     own_b.wait()
-    own_x.wait()
     b_msg(z, 0, 1, NZ - 1).start()
     b_msg(z, 8, 2, 1).start()
-    x_msg(z, 0, 1, NZ - 1).start()
-    x_msg(z, 7, 2, 1).start()
+    own_bias.wait()
+    own_gain.wait()
+    for small in x_msgs(z, 0, 1, NZ - 1) + x_msgs(z, 7, 2, 1):
+        small.start()
     for j in (1, 2, 3):
         b2_send(0, j).start()
-    lax.fori_loop(2, STEPS, start_v, 0)
+    lax.fori_loop(0, STEPS, start_own_v, 0)
     own_gate.start()
 
     own_seg.wait()
@@ -253,21 +292,24 @@
         @pl.when((k >= 1) & (k <= 6))
         def _():
             a_msg(zh, k, k, 1).wait_recv()
-            x_msg(zh, k, k, 1).wait_recv()
+            for small in x_msgs(zh, k, k, 1):
+                small.wait_recv()
             b_msg(zh, k, k, 1).wait_recv()
 
         @pl.when((k >= 1) & (k <= 4))
         def _():
             dz = jnp.where(odd, NZ - 1, 1)
             a_msg(zh, k, k + 2, dz).start()
-            x_msg(zh, k, k + 2, dz).start()
+            for small in x_msgs(zh, k, k + 2, dz):
+                small.start()
             b_msg(zh, k, k + 2, dz).start()
 
         @pl.when(k == 5)
         def _():
             a_half(zh, 0, 5, 7, NZ - 1).start()
             b_half(zh, 0, 5, 7, NZ - 1).start()
-            x_msg(zh, 5, 7, NZ - 1).start()
+            for small in x_msgs(zh, 5, 7, NZ - 1):
+                small.start()
 
         @pl.when(k == 6)
         def _():
@@ -278,7 +320,8 @@
         def _():
             a_half(zh, 0, 7, 7, 1).wait_recv()
             a_half(zh, 2, 7, 8, 1).wait_recv()
-            x_msg(zh, 7, 7, 1).wait_recv()
+            for small in x_msgs(zh, 7, 7, 1):
+                small.wait_recv()
             b_half(zh, 0, 7, 7, 1).wait_recv()
             b_half(zh, HALF // 2, 7, 8, 1).wait_recv()
 
@@ -297,10 +340,10 @@
         own_v(k).wait()
         for j in (1, 2, 3):
             v_recv(k, j).wait_recv()
-        aux = aux_buf[zh]
-        gain = aux[:, BLK:]
+        gain = gain_buf[zh].astype(F32)
+        bias = bias_buf[zh].astype(F32)
         for t in range(BLK // TOK):
-            col_buf[pl.ds(t * TOK, TOK), :] = as_column(aux[:, t * TOK : (t + 1) * TOK])
+            col_buf[pl.ds(t * TOK, TOK), :] = as_column(bias[:, t * TOK : (t + 1) * TOK])
 
         def norm_rows(i, carry):
             rows = pl.ds(pl.multiple_of(i * 128, 128), 128)
@@ -389,17 +432,17 @@
         a_half(z, 0, k, 0, 1).wait_send()
         b_half(z, 0, k, 0, 1).wait_send()
     for k in (0, 1, 2, 3, 4, 5, 7):
-        x_msg(z, k, 0, 1).wait_send()
+        for small in x_msgs(z, k, 0, 1):
+            small.wait_send()
 
 
 def per_device(gate_in, value_in, segments, value_gain, mixing, mixing_bias):
-    aux = jnp.concatenate([mixing_bias.astype(F32), value_gain.astype(F32)[None, :]], axis=1)
     any_space = pl.BlockSpec(memory_space=pl.ANY)
     dma = pltpu.SemaphoreType.DMA
     return pl.pallas_call(
         kernel,
-        out_shape=jax.ShapeDtypeStruct(value_in.shape, BF16),
-        in_specs=[any_space] * 5,
+        out_shape=pltpu.VMEM(value_in.shape, BF16),
+        in_specs=[any_space] * 6,
         out_specs=pl.BlockSpec(memory_space=pltpu.VMEM),
         scratch_shapes=[
             pltpu.VMEM((NZ, NY, NC, 2, HALF, BLK), BF16),
@@ -411,8 +454,9 @@
             pltpu.VMEM((NX * TOK, HD), BF16),
             pltpu.VMEM((BLK, HD), F32),
             pltpu.VMEM((NX, 1, TOK), jnp.int32),
-            pltpu.VMEM((NZ, 1, BLK + HD), F32),
-            dma((5,)),
+            pltpu.VMEM((NZ, 1, BLK), BF16),
+            pltpu.VMEM((NZ, 1, HD), BF16),
+            dma((6,)),
             dma((STEPS,)),
             dma((3,)),
             dma((3,)),
@@ -428,15 +472,19 @@
             dma((9,)),
             dma((8,)),
             dma((8,)),
+            dma((8,)),
+            dma((8,)),
             dma((STEPS, 3)),
             dma((STEPS, 3)),
             dma((STEPS,)),
             dma((STEPS,)),
+            pltpu.SemaphoreType.REGULAR,
+            pltpu.SemaphoreType.REGULAR,
         ],
         compiler_params=pltpu.CompilerParams(
-            collective_id=0, has_side_effects=True, vmem_limit_bytes=60 * 1024 * 1024
+            collective_id=0, has_side_effects=True, vmem_limit_bytes=48 * 1024 * 1024
         ),
-    )(gate_in, value_in, segments, aux, mixing)
+    )(*(pltpu.with_memory_space_constraint(a, pltpu.HBM) for a in (gate_in, value_in, segments, value_gain.reshape(1, HD), mixing, mixing_bias)))
 
 
 def solution(mesh):

time: 110 us -> 101 us (0.918)
  Pallas kernels: 102 us -> 98.1 us
  local copies, waits for them, and re-layouts: 4.7 us -> 2.02 us
  other arithmetic: 1.3 us -> 0 us
    pallas_call x1, Pallas kernels: 102 us -> 98.1 us  [per_device(): pl.pallas_call(kernel, out_shape=pltpu.VMEM(value_in.shape, BF16), in_spe...]
    unnamed x1, local copies, waits for them, and re-layouts: 4.7 us -> 2.02 us
    concatenate x1 -> x0, other arithmetic: 1.3 us -> none  [per_device(): jnp.concatenate([mixing_bias.astype(F32), value_gain.astype(F32)[None, :]...]
where the time goes in v2:
time: 101 us; the launch traced here: 100 us
  Pallas kernels  98.1 us (97%)
  local copies, waits for them, and re-layouts  2.02 us (2%)
    pallas_call x1, Pallas kernels, per_device(): pl.pallas_call(kernel, out_shape=pltpu.VMEM(value_in.shape, BF16), in_spe...  98.1 us

profile of v2, /device:TPU:6, one launch (start us, length us, event | category | flops | bytes accessed | tf_op | source)
XLA Modules:
  0.0 100.1 jit_solution(15395996265157984614)
XLA Ops:
  0.0 98.1 %shard_map.64 = bf16[1,512,4096]{2,1,0:T(8,128)(2,1)S(1)} custom-call(bf16[1,512,4096]{2,1,0:T(8,128)(2,1)} %gate_hbm.1, bf16[1,512,4096]{2,1,0:T(8,128)(2,1)} %value_hbm.1, s32[1,512]{1,0:T(1,128)} %seg_hbm.1, bf16[1,128]{1,0:T(2,128)(2,1)} %bitcast.1, bf16[1,128,1024]{2,1,0:T(8,128)(2,1)} %mix_hbm.1, bf16[1,1024]{1,0:T(2,128)(2,1)} %bias_hbm.1), custom_call_target="tpu_custom_call" | custom-call | tf_op jit(solution)/shard_map/pallas_call | solution.py:442
  98.1 2.0 %copy.8 = bf16[1,512,4096]{2,1,0:T(8,128)(2,1)} copy(bf16[1,512,4096]{2,1,0:T(8,128)(2,1)S(1)} %shard_map.64) | data formatting | bytes 8388608

commit v3 on v2

--- a/solution.py
+++ b/solution.py
@@ -14,6 +14,7 @@
 BLK = 1024
 HALF = 64
 STEPS = 8
+INBOX_X = 0
 
 
 def gelu(x):
@@ -137,12 +138,8 @@
         ref = m_buf.at[z, lax.rem(y + NY - j, NY), c, 0]
         return remote(ref, ref, a1_s.at[j - 1], a1_r.at[j - 1], y_peer(j))
 
-    def a_msg(zh, ss, rs, dz):
-        ref = m_buf.at[zh, :, c, 0]
-        return remote(ref, ref, a_s.at[ss], a_r.at[rs], z_peer(dz))
-
-    def a_half(zh, lo, ss, rs, dz):
-        ref = m_buf.at[zh, pl.ds(lo, 2), c, 0]
+    def a_msg(zh, half, ss, rs, dz):
+        ref = m_buf.at[zh, pl.ds(2 * half, 2), c, 0]
         return remote(ref, ref, a_s.at[ss], a_r.at[rs], z_peer(dz))
 
     def b_msg(zh, ss, rs, dz):
@@ -177,19 +174,48 @@
         return remote(ref, ref, c_s.at[k], c_r.at[k], sibling)
 
     barrier = pltpu.get_barrier_semaphore()
-
-    def tell(peer, core):
-        there = {"sp": peer["sp"], "dp": peer["dp"] // NC * NC + core}
+    inbox = (x == INBOX_X) & (c == 0)
+    helper = (x == INBOX_X) & (c == 1)
+
+    for j in (1, 2, 3):
+        to_inbox = (lax.rem(x + j, NX) == INBOX_X) & (c == 0)
+        there = {"sp": x_peer(j)["sp"], "dp": jnp.where(to_inbox, dp + 1, dp)}
         pl.semaphore_signal(barrier, inc=1, device_id=there, device_id_type=MESH)
 
-    @pl.when(c == 0)
+    @pl.when(inbox)
     def _():
         pl.semaphore_signal(barrier, inc=1, device_id=sibling, device_id_type=MESH)
 
-    for j in (1, 2, 3):
-        tell(x_peer(j), 1)
-    for peer in [z_peer(1), z_peer(NZ - 1)] + [y_peer(j) for j in (1, 2, 3)]:
-        tell(peer, 0)
+    for far_z, far_y in [(lax.rem(z + j, NZ), y) for j in (1, NZ - 1)] + [
+        (z, lax.rem(y + j, NY)) for j in (1, 2, 3)
+    ]:
+        pl.semaphore_signal(
+            barrier,
+            inc=1,
+            device_id={"sp": far_z * NX + INBOX_X, "dp": far_y * NC},
+            device_id_type=MESH,
+        )
+    @pl.when(jnp.logical_not(inbox))
+    def _():
+        pl.semaphore_wait(barrier, jnp.where(helper, 7, 3))
+
+    @pl.when(helper)
+    def _():
+        pl.semaphore_signal(row_sem, inc=1, device_id=sibling, device_id_type=MESH)
+
+    @pl.when(inbox)
+    def _():
+        pl.semaphore_wait(row_sem, 1)
+
+    def start_v(k, carry):
+        for j in (1, 3, 2):
+            v_send(k, j).start()
+        return carry
+
+    for j in (1, 2, 3):
+        seg_send(j).start()
+    lax.fori_loop(0, STEPS, start_v, 0)
+
 
     own_a = pltpu.make_async_copy(mix_hbm.at[0, pl.ds(0, HALF)], m_buf.at[z, y, c, 0], loc_sem.at[0])
     own_b = pltpu.make_async_copy(mix_hbm.at[0, pl.ds(HALF, HALF)], m_buf.at[z, y, c, 1], loc_sem.at[1])
@@ -206,37 +232,22 @@
     for own in (own_b, own_a, own_bias, own_gain, own_seg):
         own.start()
 
-    @pl.when(c == 1)
+    @pl.when(inbox)
     def _():
-        pl.semaphore_wait(barrier, 7)
-        pl.semaphore_signal(row_sem, inc=1, device_id=sibling, device_id_type=MESH)
-
-    @pl.when(c == 0)
+        pl.semaphore_wait(barrier, 5 * NX * NC)
+        for j in range(NX):
+            for core in range(NC):
+                if j or core:
+                    there = {"sp": x_peer(j)["sp"], "dp": y * NC + core}
+                    pl.semaphore_signal(far_sem, inc=1, device_id=there, device_id_type=MESH)
+
+    @pl.when(jnp.logical_not(inbox))
     def _():
-        pl.semaphore_wait(row_sem, 1)
-
-    def start_v(k, carry):
-        for j in (1, 3, 2):
-            v_send(k, j).start()
-        return carry
+        pl.semaphore_wait(far_sem, 1)
 
     def start_own_v(k, carry):
         own_v(k).start()
         return carry
-
-    lax.fori_loop(0, 1, start_v, 0)
-    for j in (1, 2, 3):
-        seg_send(j).start()
-    lax.fori_loop(1, STEPS, start_v, 0)
-
-    @pl.when(c == 0)
-    def _():
-        pl.semaphore_wait(barrier, 10)
-        pl.semaphore_signal(far_sem, inc=1, device_id=sibling, device_id_type=MESH)
-
-    @pl.when(c == 1)
-    def _():
-        pl.semaphore_wait(far_sem, 1)
 
     for j in (1, 2, 3):
         a1_send(j).start()
@@ -277,66 +288,64 @@
 
             lax.fori_loop(0, BLK // 64, mask_rows, 0)
 
-    def serve(k):
+    def ways(k):
+        return NZ - 1 if k % 2 else 1
+
+    def serve_second(k):
         zh = head_z(k)
-        odd = lax.rem(k, 2) == 1
-
-        @pl.when(k == 0)
-        def _():
-            own_a.wait()
-            for j in (1, 2, 3):
-                a1_recv(j).wait_recv()
-            a_msg(z, 0, 1, NZ - 1).start()
-            a_msg(z, 8, 2, 1).start()
-
-        @pl.when((k >= 1) & (k <= 6))
-        def _():
-            a_msg(zh, k, k, 1).wait_recv()
-            for small in x_msgs(zh, k, k, 1):
-                small.wait_recv()
+        for small in x_msgs(zh, k, k, 1):
+            small.wait_recv()
+        if k < 7:
             b_msg(zh, k, k, 1).wait_recv()
-
-        @pl.when((k >= 1) & (k <= 4))
-        def _():
-            dz = jnp.where(odd, NZ - 1, 1)
-            a_msg(zh, k, k + 2, dz).start()
-            for small in x_msgs(zh, k, k + 2, dz):
-                small.start()
-            b_msg(zh, k, k + 2, dz).start()
-
-        @pl.when(k == 5)
-        def _():
-            a_half(zh, 0, 5, 7, NZ - 1).start()
-            b_half(zh, 0, 5, 7, NZ - 1).start()
-            for small in x_msgs(zh, 5, 7, NZ - 1):
-                small.start()
-
-        @pl.when(k == 6)
-        def _():
-            a_half(zh, 2, 6, 8, 1).start()
-            b_half(zh, HALF // 2, 6, 8, 1).start()
-
-        @pl.when(k == 7)
-        def _():
-            a_half(zh, 0, 7, 7, 1).wait_recv()
-            a_half(zh, 2, 7, 8, 1).wait_recv()
-            for small in x_msgs(zh, 7, 7, 1):
-                small.wait_recv()
+        else:
             b_half(zh, 0, 7, 7, 1).wait_recv()
             b_half(zh, HALF // 2, 7, 8, 1).wait_recv()
-
-        @pl.when(k >= 1)
-        def _():
-            for j in (1, 2, 3):
-                b2_send(k, j).start()
+        if k <= 4:
+            b_msg(zh, k, k + 2, ways(k)).start()
+        elif k == 5:
+            b_half(zh, 0, 5, 7, ways(k)).start()
+        elif k == 6:
+            b_half(zh, HALF // 2, 6, 8, ways(k)).start()
+        if k <= 5:
+            for small in x_msgs(zh, k, k + 2, ways(k)):
+                small.start()
+        for j in (1, 2, 3):
+            b2_send(k, j).start()
+
+    def serve_first(k, half):
+        zh = head_z(k)
+        a_msg(zh, half, 0, 2 * k + half, 1).wait_recv()
+        if k <= 4 or k == 5 + half:
+            to = 2 * (k + 2) + half if k <= 4 else 14 + half
+            a_msg(zh, half, 2 * k + half, to, ways(k)).start()
 
     def across(k):
         for j in (1, 2, 3):
             b2_recv(k, j).wait_recv()
         c_send(k).start()
 
+    for k in (1, 2):
+        serve_second(k)
+    own_a.wait()
+    for j in (1, 2, 3):
+        a1_recv(j).wait_recv()
+    for half in (0, 1):
+        a_msg(z, half, half, 2 + half, NZ - 1).start()
+        a_msg(z, half, 14 + half, 4 + half, 1).start()
+    for k in (3, 4, 5, 6):
+        serve_second(k)
+    across(0)
+    serve_second(7)
+
     def compute(k):
         zh = head_z(k)
+        for pair in (2, 3):
+
+            @pl.when(k == 2 * pair - 2)
+            def _():
+                serve_first(2 * pair - 1, 0)
+                serve_first(2 * pair, 0)
+
         own_v(k).wait()
         for j in (1, 2, 3):
             v_recv(k, j).wait_recv()
@@ -353,6 +362,12 @@
             return carry
 
         lax.fori_loop(0, NX * TOK // 128, norm_rows, 0)
+
+        @pl.when(k == 0)
+        def _():
+            serve_first(1, 0)
+            serve_first(2, 0)
+
         c_recv(k).wait_recv()
 
         def mix_rows(i, carry):
@@ -370,22 +385,47 @@
         for j in (1, 3, 2):
             r_send(k, j).start()
 
-    def step(i, carry):
-        @pl.when(i < STEPS)
+    def step(k, carry):
+        compute(k)
+        for pair in (1, 2, 3):
+
+            @pl.when(k == 2 * pair - 2)
+            def _():
+                serve_first(2 * pair - 1, 1)
+                serve_first(2 * pair, 1)
+                across(2 * pair - 1)
+                across(2 * pair)
+
+        @pl.when(k == 5)
         def _():
-            serve(i)
-
-        @pl.when((i >= 1) & (i <= STEPS))
-        def _():
-            across(i - 1)
-
-        @pl.when(i >= 2)
-        def _():
-            compute(i - 2)
+            serve_first(7, 0)
+            serve_first(7, 1)
+            across(7)
 
         return carry
 
-    lax.fori_loop(0, STEPS + 2, step, 0)
+    lax.fori_loop(0, STEPS, step, 0)
+
+    def sent(k, carry):
+        for j in (1, 2, 3):
+            v_send(k, j).wait_send()
+            b2_send(k, j).wait_send()
+        c_send(k).wait_send()
+        return carry
+
+    lax.fori_loop(0, STEPS, sent, 0)
+    for j in (1, 2, 3):
+        seg_send(j).wait_send()
+        a1_send(j).wait_send()
+    for k in (0, 1, 2, 3, 4, 5, 6, 7, 8, 9, 10, 13, 14, 15):
+        a_msg(z, 0, k, 0, 1).wait_send()
+    for k in (0, 1, 2, 3, 4, 8):
+        b_msg(z, k, 0, 1).wait_send()
+    for k in (5, 6):
+        b_half(z, 0, k, 0, 1).wait_send()
+    for k in (0, 1, 2, 3, 4, 5, 7):
+        for small in x_msgs(z, k, 0, 1):
+            small.wait_send()
 
     own_gate.wait()
 
@@ -409,31 +449,11 @@
             r_recv(k, j).wait_recv()
             xs = lax.rem(x + NX - j, NX)
             gate_rows(k, xs, lambda lo: o_buf[xs, k, pl.ds(lo, 128), :])
+        for j in (1, 3, 2):
+            r_send(k, j).wait_send()
         return carry
 
     lax.fori_loop(0, STEPS, gated, 0)
-
-    def sent(k, carry):
-        for j in (1, 2, 3):
-            v_send(k, j).wait_send()
-            r_send(k, j).wait_send()
-            b2_send(k, j).wait_send()
-        c_send(k).wait_send()
-        return carry
-
-    lax.fori_loop(0, STEPS, sent, 0)
-    for j in (1, 2, 3):
-        seg_send(j).wait_send()
-        a1_send(j).wait_send()
-    for k in (0, 1, 2, 3, 4, 8):
-        a_msg(z, k, 0, 1).wait_send()
-        b_msg(z, k, 0, 1).wait_send()
-    for k in (5, 6):
-        a_half(z, 0, k, 0, 1).wait_send()
-        b_half(z, 0, k, 0, 1).wait_send()
-    for k in (0, 1, 2, 3, 4, 5, 7):
-        for small in x_msgs(z, k, 0, 1):
-            small.wait_send()
 
 
 def per_device(gate_in, value_in, segments, value_gain, mixing, mixing_bias):
@@ -466,8 +486,8 @@
             dma((STEPS, 3)),
             dma((3,)),
             dma((3,)),
-            dma((9,)),
-            dma((9,)),
+            dma((16,)),
+            dma((16,)),
             dma((9,)),
             dma((9,)),
             dma((8,)),

time: 101 us -> 100 us (0.990)
  no operation moved by 1% of the time
where the time goes in v3:
time: 100 us; the launch traced here: 99.4 us
  Pallas kernels  97.4 us (97%)
  local copies, waits for them, and re-layouts  2.02 us (2%)
    pallas_call x1, Pallas kernels, per_device(): pl.pallas_call(kernel, out_shape=pltpu.VMEM(value_in.shape, BF16), in_spe...  97.4 us
    unnamed x1, local copies, waits for them, and re-layouts  2.02 us

profile of v3, /device:TPU:6, one launch (start us, length us, event | category | flops | bytes accessed | tf_op | source)
XLA Modules:
  0.0 99.4 jit_solution(6702430364149713604)
XLA Ops:
  0.0 97.4 %shard_map.64 = bf16[1,512,4096]{2,1,0:T(8,128)(2,1)S(1)} custom-call(bf16[1,512,4096]{2,1,0:T(8,128)(2,1)} %gate_hbm.1, bf16[1,512,4096]{2,1,0:T(8,128)(2,1)} %value_hbm.1, s32[1,512]{1,0:T(1,128)} %seg_hbm.1, bf16[1,128]{1,0:T(2,128)(2,1)} %bitcast.1, bf16[1,128,1024]{2,1,0:T(8,128)(2,1)} %mix_hbm.1, bf16[1,1024]{1,0:T(2,128)(2,1)} %bias_hbm.1), custom_call_target="tpu_custom_call" | custom-call | tf_op jit(solution)/shard_map/pallas_call | solution.py:462
  97.4 2.0 %copy.8 = bf16[1,512,4096]{2,1,0:T(8,128)(2,1)} copy(bf16[1,512,4096]{2,1,0:T(8,128)(2,1)S(1)} %shard_map.64) | data formatting | bytes 8388608

commit v4 on v3

--- a/solution.py
+++ b/solution.py
@@ -208,13 +208,20 @@
         pl.semaphore_wait(row_sem, 1)
 
     def start_v(k, carry):
-        for j in (1, 3, 2):
+        for j in (1, 3):
             v_send(k, j).start()
         return carry
 
     for j in (1, 2, 3):
         seg_send(j).start()
-    lax.fori_loop(0, STEPS, start_v, 0)
+    def start_far_v(k, carry):
+        v_send(k, 2).start()
+        return carry
+
+    lax.fori_loop(0, 2, start_far_v, 0)
+    lax.fori_loop(0, 1, start_v, 0)
+    lax.fori_loop(2, STEPS, start_far_v, 0)
+    lax.fori_loop(1, STEPS, start_v, 0)
 
 
     own_a = pltpu.make_async_copy(mix_hbm.at[0, pl.ds(0, HALF)], m_buf.at[z, y, c, 0], loc_sem.at[0])

time: 100 us -> 99.7 us (level)
  no operation moved by 1% of the time
where the time goes in v4:
time: 99.7 us; the launch traced here: 98.7 us
  Pallas kernels  96.7 us (97%)
  local copies, waits for them, and re-layouts  2.02 us (2%)
    pallas_call x1, Pallas kernels, per_device(): pl.pallas_call(kernel, out_shape=pltpu.VMEM(value_in.shape, BF16), in_spe...  96.7 us
    unnamed x1, local copies, waits for them, and re-layouts  2.02 us

profile of v4, /device:TPU:6, one launch (start us, length us, event | category | flops | bytes accessed | tf_op | source)
XLA Modules:
  0.0 98.7 jit_solution(16220573793836275343)
XLA Ops:
  0.0 96.7 %shard_map.64 = bf16[1,512,4096]{2,1,0:T(8,128)(2,1)S(1)} custom-call(bf16[1,512,4096]{2,1,0:T(8,128)(2,1)} %gate_hbm.1, bf16[1,512,4096]{2,1,0:T(8,128)(2,1)} %value_hbm.1, s32[1,512]{1,0:T(1,128)} %seg_hbm.1, bf16[1,128]{1,0:T(2,128)(2,1)} %bitcast.1, bf16[1,128,1024]{2,1,0:T(8,128)(2,1)} %mix_hbm.1, bf16[1,1024]{1,0:T(2,128)(2,1)} %bias_hbm.1), custom_call_target="tpu_custom_call" | custom-call | tf_op jit(solution)/shard_map/pallas_call | solution.py:469
  96.7 2.0 %copy.8 = bf16[1,512,4096]{2,1,0:T(8,128)(2,1)} copy(bf16[1,512,4096]{2,1,0:T(8,128)(2,1)S(1)} %shard_map.64) | data formatting | bytes 8388608

commit v5 on v4

--- a/solution.py
+++ b/solution.py
@@ -220,8 +220,10 @@
 
     lax.fori_loop(0, 2, start_far_v, 0)
     lax.fori_loop(0, 1, start_v, 0)
-    lax.fori_loop(2, STEPS, start_far_v, 0)
-    lax.fori_loop(1, STEPS, start_v, 0)
+    lax.fori_loop(2, 5, start_far_v, 0)
+    lax.fori_loop(1, 2, start_v, 0)
+    lax.fori_loop(5, STEPS, start_far_v, 0)
+    lax.fori_loop(2, STEPS, start_v, 0)
 
 
     own_a = pltpu.make_async_copy(mix_hbm.at[0, pl.ds(0, HALF)], m_buf.at[z, y, c, 0], loc_sem.at[0])

time: 99.7 us -> 99.8 us (level)
  no operation moved by 1% of the time
where the time goes in v5:
time: 99.8 us; the launch traced here: 98.7 us
  Pallas kernels  96.7 us (97%)
  local copies, waits for them, and re-layouts  2.02 us (2%)
    pallas_call x1, Pallas kernels, per_device(): pl.pallas_call(kernel, out_shape=pltpu.VMEM(value_in.shape, BF16), in_spe...  96.7 us
    unnamed x1, local copies, waits for them, and re-layouts  2.02 us

profile of v5, /device:TPU:6, one launch (start us, length us, event | category | flops | bytes accessed | tf_op | source)
XLA Modules:
  0.0 98.7 jit_solution(4394275688845234233)
XLA Ops:
  0.0 96.7 %shard_map.64 = bf16[1,512,4096]{2,1,0:T(8,128)(2,1)S(1)} custom-call(bf16[1,512,4096]{2,1,0:T(8,128)(2,1)} %gate_hbm.1, bf16[1,512,4096]{2,1,0:T(8,128)(2,1)} %value_hbm.1, s32[1,512]{1,0:T(1,128)} %seg_hbm.1, bf16[1,128]{1,0:T(2,128)(2,1)} %bitcast.1, bf16[1,128,1024]{2,1,0:T(8,128)(2,1)} %mix_hbm.1, bf16[1,1024]{1,0:T(2,128)(2,1)} %bias_hbm.1), custom_call_target="tpu_custom_call" | custom-call | tf_op jit(solution)/shard_map/pallas_call | solution.py:471
  96.7 2.0 %copy.8 = bf16[1,512,4096]{2,1,0:T(8,128)(2,1)} copy(bf16[1,512,4096]{2,1,0:T(8,128)(2,1)S(1)} %shard_map.64) | data formatting | bytes 8388608
